TPU v7x, 128 devices: a whole 4x4x4 slice. The times are simulated.
128 devices in a mesh: sp: 32 (over z, y, core), tp: 4 (over x).
Axes of the slice: x: 4, y: 4, z: 4, core: 2. Of those that a mesh axis runs over, the one named last changes fastest.
Arguments:
- residual_input_stream: bfloat16 [24576, 2048], P('sp'), may hold values from -6 to 6
- projected_queries: bfloat16 [24576, 512], P('sp', 'tp'), may hold values from -6 to 6
- projected_keys: bfloat16 [24576, 512], P('sp', 'tp'), may hold values from -6 to 6
- projected_values: bfloat16 [24576, 1024], P('sp', 'tp'), may hold values from -6 to 6
- emitted_switch_entries: bfloat16 [24576, 1024], P('sp', 'tp'), may hold values from -6 to 6
- retention_preactivations: bfloat16 [24576, 512], P('sp', 'tp'), may hold values from -6 to 15
- additional_fading_amount: float32 [24576], P('sp'), may hold values from -2 to 0
- head_norm_gain: float32 [128], replicated, may hold values from 0.1 to 1.9
- attention_output_weight: bfloat16 [1024, 2048], P('tp'), may hold values from -0.1875 to 0.1875
- feedforward_norm_gain: float32 [2048], replicated, may hold values from 0.1 to 1.9
- gate_up_matrix: bfloat16 [2048, 5632], P('sp', 'tp'), may hold values from -0.125 to 0.125
- value_up_matrix: bfloat16 [2048, 5632], P('sp', 'tp'), may hold values from -0.125 to 0.125
- gate_filter_taps: bfloat16 [3, 5632], P(None, 'tp'), may hold values from -3.5 to 3.5
- value_filter_taps: bfloat16 [3, 5632], P(None, 'tp'), may hold values from -3.5 to 3.5
- down_projection_weight: bfloat16 [5632, 2048], P('tp', 'sp'), may hold values from -0.078125 to 0.078125
Outputs:
- layer_out: bfloat16 [24576, 2048], P(('sp', 'tp'))
All inputs are finite; a program needn't handle non-finite values.
Results may differ from a plain program's by a relative error of at most 0.011.
Values may be sent and summed in bfloat16 or wider, within the bound.
A program may use at most 128 MiB of HBM per device.

v0:
```python
import jax
import jax.numpy as jnp
from jax import lax
from jax.sharding import Mesh
from jax.sharding import PartitionSpec as P

DK = 64
DV = 128
CONV = 3
BLOCK = 64
SP = ("sp_0", "sp_1", "sp_2")
SP_TP = ("sp_0", "sp_1", "sp_2", "tp")


eps = 1e-06
retention_sharpness = 16.0


def laid_out(pieces, dim):
    pieces = jnp.moveaxis(pieces, 0, dim)
    dims = pieces.shape
    return pieces.reshape(*dims[:dim], dims[dim] * dims[dim + 1], *dims[dim + 2 :])


def copy_for_each(array, axis):
    size = lax.axis_size(axis)
    return lax.all_to_all(
        jnp.broadcast_to(array[None], (size, *array.shape)), axis, 0, 0, tiled=True
    )


def gather_directly(array, axis, dim):
    return laid_out(copy_for_each(array, axis), dim)


def filled_with(array, identity):
    return jax.tree.map(
        lambda part, zero: jnp.zeros_like(part) + jnp.asarray(zero, part.dtype), array, identity
    )


def all_in_one(array, axis):
    leaves = jax.tree.leaves(array)
    order = sorted(range(len(leaves)), key=lambda k: -leaves[k].size)
    width = (1, *leaves[order[0]].shape)[-1]
    lines = [
        jnp.pad(leaves[k].reshape(-1), (0, -leaves[k].size % width)).reshape(-1, width)
        for k in order
    ]
    both, at, found = (lax.all_gather(jnp.concatenate(lines), axis), 0, {})
    for k, line in zip(order, lines):
        share = both[:, at : at + len(line)].reshape(len(both), -1)
        found[k] = share[:, : leaves[k].size].reshape(-1, *leaves[k].shape)
        at += len(line)
    numbers = iter(range(len(leaves)))
    return jax.tree.map(lambda _: found[next(numbers)], array)


def entering(array, axes, combine, identity):
    before = start = filled_with(array, identity)
    subtotal = array
    for axis in reversed(axes):
        size, mine = (lax.axis_size(axis), lax.axis_index(axis))
        pieces = all_in_one(subtotal, axis)
        inside, subtotal = (start, start)
        for k in range(size):
            passed = k < mine
            subtotal = combine(subtotal, jax.tree.map(lambda part: part[k], pieces))
            inside = jax.tree.map(lambda new, old: jnp.where(passed, new, old), subtotal, inside)
        before = combine(inside, before)
    return before


def in_one_piece(arrays, axis, dim, along):
    both = jnp.concatenate(arrays, axis=along)
    out, at, outs = (lax.all_gather(both, axis, axis=dim, tiled=True), 0, [])
    for a in arrays:
        outs.append(lax.slice_in_dim(out, at, at + a.shape[along], axis=along))
        at += a.shape[along]
    return tuple(outs)


def from_behind(block, axis, distance):
    devices = range(lax.axis_size(axis))
    route = [(i - distance, i) for i in devices if i - distance in devices]
    return lax.ppermute(block, axis, route)


def all_blocks(array, axes, order):
    pieces = array[None]
    for k in order:
        pieces = lax.all_gather(pieces, axes[k], axis=0, tiled=True)
    held = [lax.axis_size(axes[k]) for k in reversed(order)]
    pieces = pieces.reshape(*held, *array.shape)
    turned = sorted(range(len(order)), key=lambda place: order[len(order) - 1 - place])
    return pieces.transpose(*turned, *range(len(order), pieces.ndim)).reshape(-1, *array.shape)


def whole_of(array, axes, order, dim):
    return laid_out(all_blocks(array, axes, order), dim)


def split_up(array, dim, size):
    before, after = (array.shape[:dim], array.shape[dim + 1 :])
    return jnp.moveaxis(array.reshape(*before, size, -1, *after), dim, 0)


def summed_on_arrival(array, axis, dim):
    size = lax.axis_size(axis)
    pieces = lax.all_to_all(split_up(array, dim, size), axis, 0, 0, tiled=True)
    return jnp.sum(pieces.astype(jnp.float32), axis=0)


def to_blocks(tensor, local_heads, width):
    count = tensor.shape[0] // BLOCK
    return tensor.astype(jnp.float32).reshape(count, BLOCK, local_heads, width)


def row_norm(stream, gain):
    scaled = stream * lax.rsqrt(jnp.mean(stream * stream, axis=-1, keepdims=True) + eps)
    return (scaled * gain).astype(jnp.bfloat16)


def depthwise(upward, before, taps):
    length = upward.shape[0]
    padded = jnp.concatenate([before, upward], axis=0)
    result = jnp.zeros(upward.shape, jnp.float32)
    for offset in range(CONV):
        result = result + taps[offset].astype(jnp.float32)[None] * padded[
            offset : offset + length
        ].astype(jnp.float32)
    return result


def per_device(
    residual_input_stream,
    projected_queries,
    projected_keys,
    projected_values,
    emitted_switch_entries,
    retention_preactivations,
    additional_fading_amount,
    head_norm_gain,
    attention_output_weight,
    feedforward_norm_gain,
    gate_up_matrix,
    value_up_matrix,
    gate_filter_taps,
    value_filter_taps,
    down_projection_weight,
):
    largest_exponent = lax.Precision.HIGHEST
    tok_rows = residual_input_stream.shape[0]
    local_heads = projected_queries.shape[1] // DK
    out_full = gather_directly(attention_output_weight, "tp", 0)
    retention_logarithm = (
        jax.nn.log_sigmoid(retention_preactivations.astype(jnp.float32)) / retention_sharpness
        + additional_fading_amount[:, None]
    )
    scaled_q = to_blocks(projected_queries, local_heads, DK) * DK ** (-0.5)
    key_heads = to_blocks(projected_keys, local_heads, DK)
    value_heads = to_blocks(projected_values, local_heads, DV)
    rate_cum = jnp.cumsum(to_blocks(retention_logarithm, local_heads, DK), axis=1)
    block_total = rate_cum[:, -1]
    before_block = jnp.cumsum(block_total, axis=0) - block_total
    q_decayed = scaled_q * jnp.exp(rate_cum)
    k_growth = key_heads * jnp.exp(-rate_cum)
    fading_through_finish = key_heads * jnp.exp(block_total[:, None] - rate_cum)
    lower = jnp.tril(jnp.ones((BLOCK, BLOCK), bool))
    scores = jnp.einsum("nihk,njhk->nhij", q_decayed, k_growth, precision=largest_exponent)
    scores = jnp.where(lower[None, None], scores, 0.0)
    within = jnp.einsum("nhij,njhv->nihv", scores, value_heads, precision=largest_exponent)
    increments = jnp.einsum(
        "nchk,nchv->nhkv", fading_through_finish, value_heads, precision=largest_exponent
    )

    def advance_recurrence(state, inputs):
        factor, increment = inputs
        return (factor[..., None] * state + increment, state)

    start_state = jnp.zeros((local_heads, DK, DV), jnp.float32)
    dev_state, state_before = lax.scan(
        advance_recurrence, start_state, (jnp.exp(block_total), increments)
    )
    earlier = jnp.einsum("nchk,nhkv->nchv", q_decayed, state_before, precision=largest_exponent)
    query_shard = scaled_q * jnp.exp(rate_cum + before_block[:, None])
    dev_log = jnp.sum(block_total, axis=0)

    def compose(earlier_pair, later_pair):
        return (
            earlier_pair[0] * later_pair[0],
            later_pair[0][..., None] * earlier_pair[1] + later_pair[1],
        )

    unit = (jnp.ones((local_heads, DK), jnp.float32), start_state)
    carried = entering((jnp.exp(dev_log), dev_state), SP, compose, unit)
    arriving_state = carried[1]
    earlier_memory_share = jnp.einsum(
        "osyq,yqi->osyi", query_shard, arriving_state, precision=largest_exponent
    )
    mech_out = (within + earlier + earlier_memory_share).reshape(tok_rows, local_heads, DV)
    mech_out = (
        mech_out
        * lax.rsqrt(jnp.mean(mech_out * mech_out, axis=-1, keepdims=True) + eps)
        * head_norm_gain
    )
    mixed = (
        mech_out.reshape(tok_rows, local_heads * DV)
        * jax.nn.silu(emitted_switch_entries.astype(jnp.float32))
    ).astype(jnp.bfloat16)
    tp_count = lax.axis_size("tp")
    share = tok_rows // tp_count
    tp_index = lax.axis_index("tp")
    own_input = lax.dynamic_slice_in_dim(residual_input_stream, tp_index * share, share, 0)
    mixed_own = lax.all_to_all(mixed, "tp", split_axis=0, concat_axis=1, tiled=True)
    attended = jnp.dot(mixed_own, out_full, preferred_element_type=jnp.float32)
    resid_own = own_input.astype(jnp.float32) + attended
    normed = gather_directly(row_norm(resid_own, feedforward_norm_gain), "tp", 0)
    pieces = in_one_piece((gate_up_matrix, value_up_matrix), SP, 0, 1)
    gate_sum = jnp.dot(normed, pieces[0], preferred_element_type=jnp.float32)
    value_sum = jnp.dot(normed, pieces[1], preferred_element_type=jnp.float32)
    gate_up = gate_sum.astype(jnp.bfloat16)
    value_up = value_sum.astype(jnp.bfloat16)
    gate_prev, value_prev = from_behind(
        (gate_up[tok_rows - (CONV - 1) :], value_up[tok_rows - (CONV - 1) :]), SP, 1
    )
    gate_mix = depthwise(gate_up, gate_prev, gate_filter_taps)
    value_mix = depthwise(value_up, value_prev, value_filter_taps)
    hidden = (jax.nn.silu(gate_mix) * value_mix).astype(jnp.bfloat16)
    down_full = whole_of(down_projection_weight, (("sp_0", "sp_1"), "sp_2"), (0, 1), 1)
    feed = summed_on_arrival(
        jnp.dot(hidden, down_full, preferred_element_type=jnp.float32).astype(jnp.bfloat16), "tp", 0
    )
    return (resid_own + feed).astype(jnp.bfloat16)


def solution(mesh):
    torus = Mesh(mesh.devices.reshape(4, 4, 2, mesh.shape["tp"]), ("sp_0", "sp_1", "sp_2", "tp"))
    return jax.shard_map(
        per_device,
        mesh=torus,
        in_specs=(
            P(SP, None),
            P(SP, "tp"),
            P(SP, "tp"),
            P(SP, "tp"),
            P(SP, "tp"),
            P(SP, "tp"),
            P(SP),
            P(),
            P("tp", None),
            P(),
            P(SP, "tp"),
            P(SP, "tp"),
            P(None, "tp"),
            P(None, "tp"),
            P("tp", SP),
        ),
        out_specs=P(SP_TP, None),
        check_vma=False,
    )
```

profile of v0, /device:TPU:0, one launch (start us, length us, event | category | flops | bytes accessed | tf_op | source)
XLA Modules:
  0.0 249.5 jit_solution(11430812572905853029)
XLA Ops:
  6.5 0.7 all-gather.15.cloned.1.call-update
  7.3 1.8 pad_maximum_fusion.2
  9.1 1.2 fusion.31
  10.3 0.5 reshape.301
  10.8 0.7 fusion.15
  11.6 0.5 mul.410
  12.0 1.4 reshape.313
  13.7 3.9 %copy_multiply_fusion.2 = (f32[12,64,2,64]{3,0,1,2:T(8,128)}, f32[12,64,2,64]{3,0,1,2:T(8,128)S(1)}, f32[12,64,2,64]{3,0,1,2:T(8,128)S(1)}, f32[12,64,2,64]{3,0,1,2:T(8,128)}) fusion(f32[12,64,2,64]{3,2,1,0:T(2,128)S(1)} %mul.410, f32[12,64,2,64]{3,0,1,2:T(8,128)S(1)} %fusion.15, f32[12,2,64]{2,0,1:T(8,128)S(1)} %get-tuple-element.117, ...), kind=kLoop, calls=%fused_computation.34 | loop fusion | flops 688128 | bytes 2764800 | tf_op jit(solution)/shard_map/mul | solution.py:186
  17.6 1.0 fusion.23
  18.6 9.2 %while.13 = (s32[]{:T(128)}, f32[2,64,128]{2,1,0:T(8,128)S(1)}, f32[12,2,64,128]{3,2,1,0:T(8,128)}, f32[12,2,64]{2,0,1:T(8,128)S(1)}, f32[12,2,64,128]{3,2,1,0:T(8,128)S(1)}, /*index=5*/s32[]{:T(128)}, s32[]{:T(128)}) while((s32[]{:T(128)}, f32[2,64,128]{2,1,0:T(8,128)S(1)}, f32[12,2,64,128]{3,2,1,0:T(8,128)}, ...), condition=%wide.region_2.3_spmd.clone, body=%wide.region_1.2_spmd.clone.sunk | while | flops 65539 | bytes 329824 | solution.py:182
  18.6 0.6 bitcast_dynamic-update-slice_fusion.2
  19.4 0.6 bitcast_dynamic-update-slice_fusion.2
  20.1 0.6 bitcast_dynamic-update-slice_fusion.2
  20.9 0.6 bitcast_dynamic-update-slice_fusion.2
  21.7 0.6 bitcast_dynamic-update-slice_fusion.2
  22.4 0.6 bitcast_dynamic-update-slice_fusion.2
  23.2 0.6 bitcast_dynamic-update-slice_fusion.2
  23.9 0.6 bitcast_dynamic-update-slice_fusion.2
  24.7 0.6 bitcast_dynamic-update-slice_fusion.2
  25.5 0.6 bitcast_dynamic-update-slice_fusion.2
  26.2 0.6 bitcast_dynamic-update-slice_fusion.2
  27.0 0.6 bitcast_dynamic-update-slice_fusion.2
  27.8 1.9 all-gather.4
  29.8 12.9 %all-gather.5 = f32[4,129,128]{2,1,0:T(8,128)S(1)} all-gather(f32[1,129,128]{2,1,0:T(8,128)S(1)} %maximum_bitcast_fusion.1), channel_id=3, replica_groups=mesh['sp_0'=4,'sp_1'=4,'sp_2'=2,'tp'=4] {'sp_1'}, dimensions={0}, use_global_device_ids=true | all-gather | bytes 330240 | tf_op jit(solution)/shard_map/all_gather | solution.py:50
  43.4 15.2 %all-gather.6 = f32[4,129,128]{2,1,0:T(8,128)S(1)} all-gather(f32[1,129,128]{2,1,0:T(8,128)S(1)} %maximum_bitcast_fusion.2), channel_id=4, replica_groups=mesh['sp_0'=4,'sp_1'=4,'sp_2'=2,'tp'=4] {'sp_0'}, dimensions={0}, use_global_device_ids=true | all-gather | bytes 330240 | tf_op jit(solution)/shard_map/all_gather | solution.py:50
  59.1 2.3 convolution_bitcast_fusion.1
  61.4 1.9 convolution_select_fusion
  63.3 0.5 fusion.14
  63.9 1.5 multiply_reduce_fusion.1
  65.7 0.6 copy.97
  66.3 1.0 mul.473
  67.6 11.5 %all_to_all.31 = bf16[4,192,256]{2,1,0:T(8,128)(2,1)S(1)} all-to-all(bf16[4,192,256]{2,1,0:T(8,128)(2,1)S(1)} %bitcast.153), channel_id=1, replica_groups=mesh['sp_0'=4,'sp_1'=4,'sp_2'=2,'tp'=4] {'tp'}, dimensions={0} | all-to-all | bytes 786432 | tf_op jit(solution)/shard_map/all_to_all | solution.py:215
  79.1 2.5 %broadcast_in_dim.70 = bf16[4,256,2048]{2,1,0:T(8,128)(2,1)} broadcast(bf16[256,2048]{1,0:T(8,128)(2,1)S(1)} %copy-done.5), dimensions={1,2} | broadcast | bytes 5242880 | tf_op jit(solution)/shard_map/broadcast_in_dim | solution.py:28
  81.6 4.9 %all-to-all-start.1 = ((bf16[4,256,2048]{2,1,0:T(8,128)(2,1)}), bf16[4,256,2048]{2,1,0:T(8,128)(2,1)}, u32[]{:S(2)}, u32[]{:S(2)}) async-start(bf16[4,256,2048]{2,1,0:T(8,128)(2,1)} %broadcast_in_dim.70), calls=%async_computation.1 | async-start | bytes 8388608 | tf_op jit(solution)/shard_map/all_to_all | solution.py:27
  86.5 3.8 %copy.108 = bf16[8,8,16,1408]{3,2,1,0:T(8,128)(2,1)} copy(bf16[8,8,16,1408]{3,1,2,0:T(8,128)(2,1)} %bitcast.151) | data formatting | bytes 5767168
  90.4 39.3 %all-to-all-done.1 = bf16[4,256,2048]{2,1,0:T(8,128)(2,1)} async-done(((bf16[4,256,2048]{2,1,0:T(8,128)(2,1)}), bf16[4,256,2048]{2,1,0:T(8,128)(2,1)}, u32[]{:S(2)}, u32[]{:S(2)}) %all-to-all-start.1) | async-done | bytes 4194336 | tf_op jit(solution)/shard_map/all_to_all | solution.py:27
  129.7 3.8 %multiply_reduce_fusion = (f32[192]{0:T(256)S(1)}, f32[192,2048]{1,0:T(8,128)S(1)}) fusion(bf16[4,256,2048]{2,1,0:T(8,128)(2,1)} %all-to-all-done.1, bf16[4,192,256]{2,1,0:T(8,128)(2,1)S(1)} %all_to_all.31, bf16[768,2048]{1,0:T(8,128)(2,1)} %param.17, s32[]{:T(128)S(6)} %select_n.144), kind=kOutput, calls=%fused_computation.24 | convolution fusion | flops 806879040 | bytes 6947588 | tf_op jit(solution)/shard_map/dot_general | solution.py:216
  134.2 34.2 %all_to_all.32 = bf16[4,192,2048]{2,1,0:T(8,128)(2,1)} all-to-all(bf16[4,192,2048]{2,1,0:T(8,128)(2,1)S(1)} %broadcast_in_dim.71), channel_id=1, replica_groups=mesh['sp_0'=4,'sp_1'=4,'sp_2'=2,'tp'=4] {'tp'}, dimensions={0} | all-to-all | bytes 6291456 | tf_op jit(solution)/shard_map/all_to_all | solution.py:27
  168.4 8.5 %fusion.4 = bf16[768,1408]{1,0:T(8,128)(2,1)S(1)} fusion(bf16[768,2048]{1,0:T(8,128)(2,1)} %bitcast.146, bf16[2048,2816]{1,0:T(8,128)(2,1)} %all-gather.11.cloned.1.call-done), kind=kOutput, calls=%fused_computation.9 | convolution fusion | flops 4430266368 | bytes 11075584 | tf_op jit(solution)/shard_map/dot_general | solution.py:220
  176.9 1.4 copy-done.13
  178.3 1.3 collective-permute-start
  179.6 5.3 %fusion.7 = bf16[768,1408]{1,0:T(8,128)(2,1)S(1)} fusion(bf16[768,2048]{1,0:T(8,128)(2,1)S(1)} %bitcast.147, bf16[2048,2816]{1,0:T(8,128)(2,1)S(1)} %copy-done.17), kind=kOutput, calls=%fused_computation.10 | convolution fusion | flops 4430266368 | bytes 11075584 | tf_op jit(solution)/shard_map/dot_general | solution.py:221
  184.9 2.4 collective-permute-start.1
  187.6 4.7 %copy.101 = bf16[16,2,1408,64]{2,3,1,0:T(8,128)(2,1)S(1)} copy(bf16[16,2,1408,64]{2,0,1,3:T(8,128)(2,1)} %bitcast.144) | data formatting | bytes 11534336 | tf_op jit(solution)/shard_map/transpose | solution.py:96
  192.3 8.4 %convolution_convert_fusion = bf16[768,2048]{1,0:T(8,128)(2,1)S(1)} fusion(bf16[1408,2048]{0,1:T(8,128)(2,1)S(1)} %bitcast.145, bf16[768,1408]{1,0:T(8,128)(2,1)S(1)} %copy-done.16, bf16[768,1408]{1,0:T(8,128)(2,1)S(1)} %copy-done.14, bf16[2,1408]{1,0:T(2,128)(2,1)S(1)} %collective-permute-done.1, bf16[2,1408]{1,0:T(2,128)(2,1)S(1)} %collective-permute-done, ...), kind=kOutput, calls=%fused_computation.11 | convolution fusion | flops 4467523584 | bytes 13283328 | tf_op jit(solution)/shard_map/dot_general | solution.py:232
  200.7 40.5 %all_to_all.33 = bf16[4,192,2048]{2,1,0:T(8,128)(2,1)S(1)} all-to-all(bf16[4,192,2048]{2,1,0:T(8,128)(2,1)S(1)} %bitcast.148), channel_id=1, replica_groups=mesh['sp_0'=4,'sp_1'=4,'sp_2'=2,'tp'=4] {'tp'}, dimensions={0} | all-to-all | bytes 6291456 | tf_op jit(solution)/shard_map/all_to_all | solution.py:110
  241.3 0.6 convert_reduce_fusion
  241.9 1.1 add_convert_fusion
  (112 shorter events, 4.1 us)
Async XLA Ops:
  6.5 59.8 %copy-start = (f32[128]{0:T(128)S(1)}, f32[128]{0:T(128)}, u32[]{:S(2)}) copy-start(f32[128]{0:T(128)} %param.24) | copy-start | bytes 1540
  6.5 5.0 %copy-start.8 = (bf16[768,128]{1,0:T(8,128)(2,1)S(1)}, bf16[768,128]{1,0:T(8,128)(2,1)}, u32[]{:S(2)}) copy-start(bf16[768,128]{1,0:T(8,128)(2,1)} %param.18) | copy-start | bytes 589828
  6.5 5.5 %copy-start.9 = (bf16[768,128]{1,0:T(8,128)(2,1)S(1)}, bf16[768,128]{1,0:T(8,128)(2,1)}, u32[]{:S(2)}) copy-start(bf16[768,128]{1,0:T(8,128)(2,1)} %param.19) | copy-start | bytes 589828
  6.5 80.0 %all-gather.15.cloned.1.call-start = ((), (), s32[]{:S(2)}) async-start(), calls=%async_computation.6 | async-start | bytes 3063808 | tf_op jit(solution)/shard_map/all_gather | solution.py:92
  7.3 161.1 %all-gather.11.cloned.1.call-start = ((), (), s32[]{:S(2)}) async-start(), calls=%async_computation.4 | async-start | bytes 11894784 | tf_op jit(solution)/shard_map/all_gather | solution.py:76
  10.8 2.6 %copy-start.6 = (bf16[768,256]{1,0:T(8,128)(2,1)S(1)}, bf16[768,256]{1,0:T(8,128)(2,1)}, u32[]{:S(2)}) copy-start(bf16[768,256]{1,0:T(8,128)(2,1)} %param.20) | copy-start | bytes 1179652
  17.6 43.9 %copy-start.3 = (f32[12,64,2,64]{3,0,1,2:T(8,128)S(1)}, f32[12,64,2,64]{3,0,1,2:T(8,128)}, u32[]{:S(2)}) copy-start(f32[12,64,2,64]{3,0,1,2:T(8,128)} %get-tuple-element.119) | copy-start | bytes 1179652
  59.0 4.9 %copy-start.2 = (f32[12,64,2,64]{3,0,1,2:T(8,128)S(1)}, f32[12,64,2,64]{3,0,1,2:T(8,128)}, u32[]{:S(2)}) copy-start(f32[12,64,2,64]{3,0,1,2:T(8,128)} %get-tuple-element.111) | copy-start | bytes 1179652
  63.3 4.0 %copy-start.7 = (bf16[768,256]{1,0:T(8,128)(2,1)S(1)}, bf16[768,256]{1,0:T(8,128)(2,1)}, u32[]{:S(2)}) copy-start(bf16[768,256]{1,0:T(8,128)(2,1)} %param.21) | copy-start | bytes 1179652
  63.9 15.1 %copy-start.5 = (bf16[256,2048]{1,0:T(8,128)(2,1)S(1)}, bf16[256,2048]{1,0:T(8,128)(2,1)}, u32[]{:S(2)}) copy-start(bf16[256,2048]{1,0:T(8,128)(2,1)} %param.25) | copy-start | bytes 3145732
  81.6 48.1 %all-to-all-start.1 = ((bf16[4,256,2048]{2,1,0:T(8,128)(2,1)}), bf16[4,256,2048]{2,1,0:T(8,128)(2,1)}, u32[]{:S(2)}, u32[]{:S(2)}) async-start(bf16[4,256,2048]{2,1,0:T(8,128)(2,1)} %broadcast_in_dim.70), calls=%async_computation.1 | async-start | bytes 8388608 | tf_op jit(solution)/shard_map/all_to_all | solution.py:27
  86.5 101.1 %all-gather.13.cloned.1.call-start = ((), (), s32[]{:S(2)}) async-start(), calls=%async_computation.5 | async-start | bytes 8650752 | tf_op jit(solution)/shard_map/all_gather | solution.py:92
  90.4 43.2 %copy-start.12 = (f32[2048]{0:T(1024)S(1)}, f32[2048]{0:T(1024)}, u32[]{:S(2)}) copy-start(f32[2048]{0:T(1024)} %param.26) | copy-start | bytes 24580
  168.4 11.2 %copy-start.4 = (bf16[4,192,2048]{2,1,0:T(8,128)(2,1)S(1)}, bf16[4,192,2048]{2,1,0:T(8,128)(2,1)}, u32[]{:S(2)}) copy-start(bf16[4,192,2048]{2,1,0:T(8,128)(2,1)} %all_to_all.32) | copy-start | bytes 9437188
  168.4 11.2 %copy-start.17 = (bf16[2048,2816]{1,0:T(8,128)(2,1)S(1)}, bf16[2048,2816]{1,0:T(8,128)(2,1)}, u32[]{:S(2)}) copy-start(bf16[2048,2816]{1,0:T(8,128)(2,1)} %all-gather.11.cloned.1.call-done) | copy-start | bytes 34603012
  176.9 1.4 copy-start.13
  178.3 9.1 %copy-start.10 = (bf16[3,1408]{1,0:T(4,128)(2,1)S(1)}, bf16[3,1408]{1,0:T(4,128)(2,1)}, u32[]{:S(2)}) copy-start(bf16[3,1408]{1,0:T(4,128)(2,1)} %param.30) | copy-start | bytes 25348
  178.3 9.1 %copy-start.11 = (bf16[3,1408]{1,0:T(4,128)(2,1)S(1)}, bf16[3,1408]{1,0:T(4,128)(2,1)}, u32[]{:S(2)}) copy-start(bf16[3,1408]{1,0:T(4,128)(2,1)} %param.29) | copy-start | bytes 25348
  178.3 14.0 %collective-permute-start = (bf16[2,1408]{1,0:T(2,128)(2,1)S(1)}, bf16[2,1408]{1,0:T(2,128)(2,1)S(1)}, u32[]{:S(2)}, u32[]{:S(2)}) collective-permute-start(bf16[2,1408]{1,0:T(2,128)(2,1)S(1)} %slice.208), channel_id=1, source_target_pairs={{0,4},{4,8},{8,12},{12,16},{16,20},{20,24},{24,28},{28,32},{32,36}... | collective-permute-start | bytes 16904 | tf_op jit(solution)/shard_map/ppermute | solution.py:86
  184.9 2.5 copy-start.15
  184.9 7.3 %collective-permute-start.1 = (bf16[2,1408]{1,0:T(2,128)(2,1)S(1)}, bf16[2,1408]{1,0:T(2,128)(2,1)S(1)}, u32[]{:S(2)}, u32[]{:S(2)}) collective-permute-start(bf16[2,1408]{1,0:T(2,128)(2,1)S(1)} %slice.212), channel_id=1, source_target_pairs={{0,4},{4,8},{8,12},{12,16},{16,20},{20,24},{24,28},{28,32},{32,36}... | collective-permute-start | bytes 16904 | tf_op jit(solution)/shard_map/ppermute | solution.py:86
  187.5 4.7 %copy-start.14 = (bf16[768,1408]{1,0:T(8,128)(2,1)S(1)}, bf16[768,1408]{1,0:T(8,128)(2,1)}, u32[]{:S(2)}) copy-start(bf16[768,1408]{1,0:T(8,128)(2,1)} %copy-done.13) | copy-start | bytes 6488068
  187.5 4.7 %copy-start.16 = (bf16[768,1408]{1,0:T(8,128)(2,1)S(1)}, bf16[768,1408]{1,0:T(8,128)(2,1)}, u32[]{:S(2)}) copy-start(bf16[768,1408]{1,0:T(8,128)(2,1)} %copy-done.15) | copy-start | bytes 6488068
  200.7 42.3 %copy-start.1 = (f32[128]{0:T(128)S(1)}, f32[128]{0:T(128)}, u32[]{:S(2)}) copy-start(f32[128]{0:T(128)} %param.24) | copy-start | bytes 1540
Sparse Core Ops, SparseCore 0:
  9.5 51.0 all-gather.14
  62.9 58.9 all-gather.10
  123.6 18.1 all-gather.12
where the time goes:
time: 253 us; the launch traced here: 250 us
  blocking collectives  116 us (46%)
  waiting for transfers between devices  40.1 us (16%)
  matrix products  33.4 us (13%)
  other arithmetic  19.1 us (8%)
  local copies, waits for them, and re-layouts  18.1 us (7%)
  between operations  13.7 us (5%)
  starting transfers between devices  8.66 us (3%)
    all_to_all x1, blocking collectives, summed_on_arrival(): pieces = lax.all_to_all(split_up(array, dim, size), axis, 0, 0, tiled=True)  40.5 us
    all_to_all x1, waiting for transfers between devices, copy_for_each(): lax.all_to_all(jnp.broadcast_to(array[None], (size, *array.shape)), axis,...  39.3 us
    all_to_all x1, blocking collectives, copy_for_each(): lax.all_to_all(jnp.broadcast_to(array[None], (size, *array.shape)), axis,...  34.2 us
    all_gather x3, blocking collectives, all_in_one(): both, at, found = (lax.all_gather(jnp.concatenate(lines), axis), 0, {})  30 us
    all_to_all x1, blocking collectives, per_device(): lax.all_to_all(mixed, 'tp', split_axis=0, concat_axis=1, tiled=True)  11.5 us
    dot_general x1, matrix products, per_device(): gate_sum = jnp.dot(normed, pieces[0], preferred_element_type=jnp.float32)  8.48 us
    dot_general x1, matrix products, per_device(): jnp.dot(hidden, down_full, preferred_element_type=jnp.float32)  8.44 us
    dynamic_update_slice x12, other arithmetic, per_device(): lax.scan(advance_recurrence, start_state, (jnp.exp(block_total), incremen...  7.69 us
  transfers between devices with their start and end apart: 6, of which 1 were waited for; matrix products, arithmetic and copies ran while one was open for 24% of the time, Pallas kernels for 0%

commit v1 on v0

v1 whole, which is shorter than its diff:
```python
import jax
import jax.numpy as jnp
from jax import lax
from jax.experimental import pallas as pl
from jax.experimental.pallas import tpu as pltpu
from jax.sharding import Mesh
from jax.sharding import PartitionSpec as P

MESH = pl.DeviceIdType.MESH
BLOCK = 64
SP = ("sp_0", "sp_1", "sp_2")
EPS = 1e-06
BF = jnp.bfloat16
F32 = jnp.float32

ROWS = 768
D = 2048
HID = 1408
CH = 192
NCH = 4
NB = ROWS // BLOCK
WCOLS = 3 * HID
HALO = 16
NT = HID // 128
CHUNKS = (3, 0, 1, 2)


def wrap(v):
    return lax.rem(v + 8, 4)


def rows_of(start, size):
    return pl.ds(pl.multiple_of(start, 16), size)


def nt_dot(a, b):
    return lax.dot_general(a, b, (((1,), (1,)), ((), ())), preferred_element_type=F32)


def tn_dot(a, b):
    return lax.dot_general(a, b, (((0,), (0,)), ((), ())), preferred_element_type=F32)


def body(
    x_hbm, q_hbm, k_hbm, v_hbm, g_hbm, lr_hbm, wo_hbm, w_hbm, hg_ref, fg_ref, taps_ref,
    out_ref,
    wbuf, wobuf, xbuf, qbuf, kbuf, vbuf, gbuf, lrbuf, tst, cbs, qst, outl,
    cbuf, ybuf, zbuf, mix, normed, resid, own, hid, parts, relay, fin,
    lsem, wsend, wrecv, dsend, drecv, osend, orecv, odsend, odrecv,
    csem, ysend, yrecv, zsend, zrecv, msend, mrecv, hsem, psend, precv,
):
    z, y, c, x = (lax.axis_index(n) for n in ("sp_0", "sp_1", "sp_2", "tp"))
    sp = z * 8 + y * 2 + c
    peer = 1 - c
    spn = lax.rem(sp + 1, 32)
    spp = lax.rem(sp + 31, 32)

    def at_sp(s):
        return {"sp_0": s // 8, "sp_1": lax.rem(s, 8) // 2, "sp_2": lax.rem(s, 2), "tp": x}

    def dev(dz=None, dy=None, dc=None, dx=None):
        return {
            "sp_0": z if dz is None else dz,
            "sp_1": y if dy is None else dy,
            "sp_2": c if dc is None else dc,
            "tp": x if dx is None else dx,
        }

    def remote(src, dst, ssem, rsem, to):
        return pltpu.make_async_remote_copy(
            src_ref=src, dst_ref=dst, send_sem=ssem, recv_sem=rsem, device_id=to,
            device_id_type=MESH,
        )

    wl = pltpu.make_async_copy(w_hbm, wbuf.at[rows_of(sp * 64, 64), :], lsem.at[0])
    wol = pltpu.make_async_copy(wo_hbm, wobuf.at[rows_of(x * 256, 256), :], lsem.at[1])
    loads = [
        pltpu.make_async_copy(a, b, lsem.at[2 + i])
        for i, (a, b) in enumerate(
            ((lr_hbm, lrbuf), (k_hbm, kbuf), (v_hbm, vbuf), (q_hbm, qbuf), (g_hbm, gbuf), (x_hbm, xbuf))
        )
    ]
    wl.start()
    wol.start()
    for cp in loads:
        cp.start()

    barrier = pltpu.get_barrier_semaphore()
    partners = [dev(dc=peer), at_sp(spn), at_sp(spp)]
    partners += [dev(dx=wrap(x + 1)), dev(dx=wrap(x - 1))]
    for dlt in (1, 2, 3):
        partners += [dev(dy=wrap(y + dlt)), dev(dz=wrap(z + dlt))]
    for to in partners:
        pl.semaphore_signal(barrier, inc=1, device_id=to, device_id_type=MESH)
    pl.semaphore_wait(barrier, len(partners))

    def wgeom(t):
        first = 1 - t // 2
        second = t // 2
        s = 1 - 2 * lax.rem(t, 2)
        p = first * y + second * z
        q = first * z + second * y

        def block(pp, qq):
            zz = first * qq + second * pp
            yy = first * pp + second * qq
            return wbuf.at[rows_of((zz * 8 + yy * 2 + c) * 64 + t * 16, 16), :]

        def to_p(dlt):
            return dev(dz=wrap(z + second * dlt), dy=wrap(y + first * dlt))

        def to_q(dlt):
            return dev(dz=wrap(z + first * dlt), dy=wrap(y + second * dlt))

        return s, p, q, block, to_p, to_q

    def wcopy(t, k):
        s, p, q, block, to_p, to_q = wgeom(t)
        if k < 3:
            blk = (block(p, q), block(p, q), block(wrap(p - s), q))[k]
            to = (to_p(1), to_p(-1), to_p(s))[k]
        else:
            m, j = divmod(k - 3, 3)
            pm = wrap(p + (0, -1, 1, 2)[m])
            blk = (block(pm, q), block(pm, q), block(pm, wrap(q - s)))[j]
            to = (to_q(1), to_q(-1), to_q(s))[j]
        return remote(blk, blk, wsend.at[t, k], wrecv.at[t, k], to)

    def wdone(t, k):
        s, p, q, block, to_p, to_q = wgeom(t)
        if k < 3:
            blk = (block(wrap(p - 1), q), block(wrap(p + 1), q), block(wrap(p + 2), q))[k]
        else:
            m, j = divmod(k - 3, 3)
            pm = wrap(p + (0, -1, 1, 2)[m])
            blk = block(pm, wrap(q + (-1, 1, 2)[j]))
        return blk

    def wstep(waits, sends):
        def one(t, carry):
            for k in waits:
                blk = wdone(t, k)
                remote(blk, blk, wsend.at[t, k], wrecv.at[t, k], dev(dc=peer)).wait_recv()
                remote(blk, blk, dsend.at[t, k], drecv.at[t, k], dev(dc=peer)).start()
            for k in sends:
                wcopy(t, k).start()
            return carry

        lax.fori_loop(0, 4, one, 0)

    own_rows = wbuf.at[rows_of(sp * 64, 64), :]
    peer_rows = wbuf.at[rows_of((sp - c + peer) * 64, 64), :]

    wl.wait()
    wstep((), (0, 1))
    own_peer = remote(own_rows, own_rows, csem.at[2], csem.at[3], dev(dc=peer))
    own_peer.start()

    def ohalf(xx, cc):
        return wobuf.at[rows_of(xx * 256 + cc * 128, 128), :]

    def oquart(xx, cc, h):
        return wobuf.at[rows_of(xx * 256 + cc * 128 + h * 64, 64), :]

    xr, xl, xo = wrap(x + 1), wrap(x - 1), wrap(x + 2)
    wol.wait()
    o0 = remote(ohalf(x, c), ohalf(x, c), osend.at[0], orecv.at[0], dev(dx=xr))
    o1 = remote(ohalf(x, c), ohalf(x, c), osend.at[1], orecv.at[1], dev(dx=xl))
    o0.start()
    o1.start()

    lane = lax.broadcasted_iota(jnp.int32, (1, 128), 1)
    low = lane < 64
    ri = lax.broadcasted_iota(jnp.int32, (64, 64), 0)
    ci = lax.broadcasted_iota(jnp.int32, (64, 64), 1)
    tri = (ri >= ci).astype(F32)
    for cp in loads[:3]:
        cp.wait()

    def state_step(n, carry):
        st, cb = carry
        rows = rows_of(n * 64, 64)
        rc = jnp.dot(tri, lrbuf[rows, :], precision=lax.Precision.HIGHEST, preferred_element_type=F32)
        lrbuf[rows, :] = rc
        bt = rc[63:64, :]
        kf = (kbuf[rows, :].astype(F32) * jnp.exp(bt - rc)).astype(BF)
        pr = tn_dot(vbuf[rows, :], kf)
        tst[n] = st
        cbs[n] = jnp.broadcast_to(cb, (8, 128))
        st = jnp.exp(bt) * st + jnp.where(low, pr[:128], pr[128:])
        return st, cb + bt

    st, la = lax.fori_loop(
        0, NB, state_step, (jnp.zeros((128, 128), F32), jnp.zeros((1, 128), F32))
    )

    def put_state(ref, s_, l_):
        ref[0:128, :] = s_
        ref[128:136, :] = jnp.broadcast_to(l_, (8, 128))

    put_state(cbuf.at[0], st, la)
    cx = remote(cbuf.at[0], cbuf.at[1], csem.at[0], csem.at[1], dev(dc=peer))
    cx.start()
    for cp in loads[3:4]:
        cp.wait()

    def within_step(n, carry):
        rows = rows_of(n * 64, 64)
        rc = lrbuf[rows, :]
        qd = qbuf[rows, :].astype(F32) * 0.125 * jnp.exp(rc)
        kg = (kbuf[rows, :].astype(F32) * jnp.exp(-rc)).astype(BF)
        zero = jnp.zeros_like(qd)
        qq = jnp.concatenate([jnp.where(low, qd, zero), jnp.where(low, zero, qd)], axis=0).astype(BF)
        qst[n] = qq
        sc = nt_dot(qq, kg)
        s0 = jnp.where(ri >= ci, sc[:64], 0.0).astype(BF)
        s1 = jnp.where(ri >= ci, sc[64:], 0.0).astype(BF)
        vv = vbuf[rows, :]
        outl[rows, 0:128] = jnp.dot(s0, vv[:, :128], preferred_element_type=F32)
        outl[rows, 128:256] = jnp.dot(s1, vv[:, 128:], preferred_element_type=F32)
        return carry

    lax.fori_loop(0, 3, within_step, 0)
    cx.wait()
    other = cbuf[1, 0:128, :]
    ola = cbuf[1, 128:129, :]
    second = c == 1
    s_first = jnp.where(second, other, st)
    s_second = jnp.where(second, st, other)
    la_second = jnp.where(second, la, ola)
    pc = jnp.where(second, other, jnp.zeros_like(other))
    pc_la = jnp.where(second, ola, jnp.zeros_like(ola))
    chip = jnp.exp(la_second) * s_first + s_second
    chip_la = la + ola

    def ring_scan(buf, ssem, rsem, me, value, value_la, to, cover):
        put_state(buf.at[me], value, value_la)
        sent = [
            remote(buf.at[me], buf.at[me], ssem.at[dlt - 1], rsem.at[dlt - 1], to(wrap(me + dlt)))
            for dlt in (1, 2, 3)
        ]
        for cp in sent:
            cp.start()
        cover()
        for dlt in (1, 2, 3):
            src = buf.at[wrap(me - dlt)]
            remote(src, src, ssem.at[dlt - 1], rsem.at[dlt - 1], to(wrap(me + dlt))).wait_recv()
        tot = jnp.zeros((128, 128), F32)
        tot_la = jnp.zeros((1, 128), F32)
        pre, pre_la = tot, tot_la
        for k in range(4):
            lk = buf[k, 128:129, :]
            tot = jnp.exp(lk) * tot + buf[k, 0:128, :]
            tot_la = tot_la + lk
            passed = k < me
            pre = jnp.where(passed, tot, pre)
            pre_la = jnp.where(passed, tot_la, pre_la)
        return pre, pre_la, tot, tot_la, sent

    py, py_la, tot, tot_la, ysent = ring_scan(
        ybuf, ysend, yrecv, y, chip, chip_la, lambda k: dev(dy=k),
        lambda: lax.fori_loop(3, 6, within_step, 0),
    )
    pz, pz_la, tot, tot_la, zsent = ring_scan(
        zbuf, zsend, zrecv, z, tot, tot_la, lambda k: dev(dz=k),
        lambda: lax.fori_loop(6, 10, within_step, 0),
    )
    tin = jnp.exp(pc_la) * (jnp.exp(py_la) * pz + py) + pc

    wstep((0, 1), (2, 3, 4, 6, 7, 9, 10))
    remote(ohalf(xl, c), ohalf(xl, c), osend.at[0], orecv.at[0], dev(dx=xr)).wait_recv()
    remote(ohalf(xr, c), ohalf(xr, c), osend.at[1], orecv.at[1], dev(dx=xl)).wait_recv()
    o2 = remote(oquart(xl, c, 0), oquart(xl, c, 0), osend.at[2], orecv.at[2], dev(dx=xr))
    o3 = remote(oquart(xr, c, 1), oquart(xr, c, 1), osend.at[3], orecv.at[3], dev(dx=xl))
    o2.start()
    o3.start()
    od = [
        remote(r, r, odsend.at[i], odrecv.at[i], dev(dc=peer))
        for i, r in enumerate((ohalf(xl, c), ohalf(xr, c), oquart(xo, c, 0), oquart(xo, c, 1)))
    ]
    od[0].start()
    od[1].start()
    lax.fori_loop(10, 12, within_step, 0)
    loads[4].wait()

    mlane = pl.multiple_of(x * 256, 256)

    def mix_step(n, carry):
        rows = rows_of(n * 64, 64)
        full = (tst[n] + jnp.exp(cbs[n][0:1, :]) * tin).astype(BF)
        e = nt_dot(qst[n], full)
        got = []
        for h in range(2):
            o = outl[rows, h * 128 : h * 128 + 128] + e[h * 64 : h * 64 + 64]
            o = o * lax.rsqrt(jnp.mean(o * o, axis=-1, keepdims=True) + EPS) * hg_ref[...]
            gt = gbuf[rows, h * 128 : h * 128 + 128].astype(F32)
            got.append(o * (gt / (1.0 + jnp.exp(-gt))))
        mix[rows, pl.ds(mlane, 256)] = jnp.concatenate(got, axis=1).astype(BF)
        return carry

    def mblock(h, xx):
        return mix.at[h * CH : h * CH + CH, pl.ds(pl.multiple_of(xx * 256, 256), 256)]

    msent = []
    for h in CHUNKS:
        lax.fori_loop(h * 3, h * 3 + 3, mix_step, 0)
        for j, to in ((0, xr), (1, xl)):
            cp = remote(mblock(h, x), mblock(h, x), msend.at[h, j], mrecv.at[h, j], dev(dx=to))
            cp.start()
            msent.append(cp)

    def mwait(h, j, xx):
        remote(mblock(h, xx), mblock(h, xx), msend.at[h, j], mrecv.at[h, j], dev(dx=xr)).wait_recv()

    wstep((3, 4, 2), (5, 12, 13))
    for h in CHUNKS:
        mwait(h, 0, xl)
        mwait(h, 1, xr)
        src, to = (xl, xr) if h % 2 == 0 else (xr, xl)
        cp = remote(mblock(h, src), mblock(h, src), msend.at[h, 2], mrecv.at[h, 2], dev(dx=to))
        cp.start()
        msent.append(cp)

    wstep((6, 7, 9, 10), (8, 11))
    remote(oquart(xo, c, 0), oquart(xo, c, 0), osend.at[2], orecv.at[2], dev(dx=xr)).wait_recv()
    remote(oquart(xo, c, 1), oquart(xo, c, 1), osend.at[3], orecv.at[3], dev(dx=xl)).wait_recv()
    od[2].start()
    od[3].start()
    for i, r in enumerate((ohalf(xl, peer), ohalf(xr, peer), oquart(xo, peer, 0), oquart(xo, peer, 1))):
        remote(r, r, odsend.at[i], odrecv.at[i], dev(dc=peer)).wait_recv()
    loads[5].wait()

    def chunk_norm(h):
        r0 = h * CH

        def cols(i, ss):
            cs = pl.ds(pl.multiple_of(i * 256, 256), 256)
            a = jnp.dot(mix[r0 : r0 + CH, :], wobuf[:, cs], preferred_element_type=F32)
            a = a + xbuf[r0 : r0 + CH, cs].astype(F32)
            resid[:, cs] = a
            sq = a * a
            return ss + sq[:, :128] + sq[:, 128:]

        ss = lax.fori_loop(0, 8, cols, jnp.zeros((CH, 128), F32))
        rs = lax.rsqrt(jnp.sum(ss, axis=-1, keepdims=True) * (1.0 / D) + EPS)

        def norm(i, carry):
            cs = pl.ds(pl.multiple_of(i * 256, 256), 256)
            normed[HALO + r0 : HALO + r0 + CH, cs] = (resid[:, cs] * rs * fg_ref[:, cs]).astype(BF)
            return carry

        lax.fori_loop(0, 8, norm, 0)

        @pl.when(x == h)
        def _():
            def keep(i, carry):
                cs = pl.ds(pl.multiple_of(i * 256, 256), 256)
                own[:, cs] = resid[:, cs]
                return carry

            lax.fori_loop(0, 8, keep, 0)

    tail = normed.at[ROWS : ROWS + HALO, :]
    halo = normed.at[0:HALO, :]
    hcopy = remote(tail, halo, hsem.at[0], hsem.at[1], at_sp(spn))
    for h in CHUNKS:
        mwait(h, 2, xo)
        chunk_norm(h)
        if h == 3:
            hcopy.start()
        if h == 1:
            wstep((12, 13), (14,))
    wstep((5, 8, 11), ())
    wstep((14,), ())
    hcopy.wait()

    @pl.when(sp == 0)
    def _():
        normed[0:HALO, :] = jnp.zeros((HALO, D), BF)

    own_peer_in = remote(peer_rows, peer_rows, csem.at[2], csem.at[3], dev(dc=peer))
    own_peer_in.wait_recv()

    def dwait(t, carry):
        for k in range(15):
            blk = wdone(t, k)
            remote(blk, blk, dsend.at[t, k], drecv.at[t, k], dev(dc=peer)).wait_recv()
        return carry

    lax.fori_loop(0, 4, dwait, 0)

    half = D // 2

    def ffn_chunk(i, carry):
        off = 2 - i + 3 * (i // 2) - 2 * (i // 3)
        h = lax.rem(x + off, 4)
        r0 = h * CH
        win = rows_of(r0, CH + HALO)

        def up(j, cc):
            cs = pl.ds(pl.multiple_of(j * 256, 256), 256)
            u = jnp.dot(normed[win, :], wbuf[:, cs], preferred_element_type=F32)
            u = u.astype(BF).astype(F32)
            t0, t1, t2 = (taps_ref[a : a + 1, cs] for a in range(3))
            m = t0 * pltpu.roll(u, 2, 0) + t1 * pltpu.roll(u, 1, 0) + t2 * u
            gm = m[HALO:, :128]
            vm = m[HALO:, 128:]
            hv = gm / (1.0 + jnp.exp(-gm)) * vm
            hid[:, pl.ds(pl.multiple_of(j * 128, 128), 128)] = hv.astype(BF)
            return cc

        lax.fori_loop(0, NT, up, 0)

        def down(j, cc):
            rs_ = rows_of(j * 256, 256)
            a = nt_dot(hid[...], wbuf[rs_, 2 * HID : WCOLS])
            parts[i, :, pl.ds(pl.multiple_of(j * 256, 256), 256)] = a.astype(BF)
            return cc

        lax.fori_loop(0, 8, down, 0)

        @pl.when(i == 0)
        def _():
            remote(parts.at[0, :, 0:half], relay.at[0], psend.at[0], precv.at[0], dev(dx=xr)).start()
            remote(parts.at[0, :, half:D], relay.at[1], psend.at[1], precv.at[1], dev(dx=xl)).start()

        @pl.when(i == 1)
        def _():
            remote(parts.at[1, :, half:D], fin.at[0, :, half:D], psend.at[2], precv.at[2], dev(dx=xr)).start()

        @pl.when(i == 2)
        def _():
            remote(parts.at[2, :, 0:half], fin.at[1, :, 0:half], psend.at[3], precv.at[3], dev(dx=xl)).start()

        return carry

    lax.fori_loop(0, NCH, ffn_chunk, 0)

    def add_relay(slot, ref, base):
        def one(j, cc):
            a = pl.ds(pl.multiple_of(j * 256, 256), 256)
            b = pl.ds(pl.multiple_of(base + j * 256, 256), 256)
            parts[slot, :, b] = (parts[slot, :, b].astype(F32) + ref[:, a].astype(F32)).astype(BF)
            return cc

        lax.fori_loop(0, 4, one, 0)

    r0c = remote(parts.at[0, :, 0:half], relay.at[0], psend.at[0], precv.at[0], dev(dx=xr))
    r1c = remote(parts.at[0, :, half:D], relay.at[1], psend.at[1], precv.at[1], dev(dx=xl))
    r0c.wait_recv()
    add_relay(1, relay.at[0], 0)
    f0 = remote(parts.at[1, :, 0:half], fin.at[0, :, 0:half], psend.at[4], precv.at[4], dev(dx=xr))
    f0.start()
    r1c.wait_recv()
    add_relay(2, relay.at[1], half)
    f1 = remote(parts.at[2, :, half:D], fin.at[1, :, half:D], psend.at[5], precv.at[5], dev(dx=xl))
    f1.start()

    def sends_over(t, carry):
        for k in range(15):
            wcopy(t, k).wait_send()
            blk = wdone(t, k)
            remote(blk, blk, dsend.at[t, k], drecv.at[t, k], dev(dc=peer)).wait_send()
        return carry

    lax.fori_loop(0, 4, sends_over, 0)
    own_peer.wait_send()
    for cp in (o0, o1, o2, o3, *od, *ysent, *zsent, *msent):
        cp.wait_send()

    g0 = remote(parts.at[1, :, half:D], fin.at[0, :, half:D], psend.at[2], precv.at[2], dev(dx=xr))
    g1 = remote(parts.at[2, :, 0:half], fin.at[1, :, 0:half], psend.at[3], precv.at[3], dev(dx=xl))
    for cp in (g0, g1, f0, f1):
        cp.wait_recv()

    def last(j, cc):
        cs = pl.ds(pl.multiple_of(j * 256, 256), 256)
        a = own[:, cs] + parts[3, :, cs].astype(F32)
        a = a + (fin[0, :, cs].astype(F32) + fin[1, :, cs].astype(F32))
        out_ref[:, cs] = a.astype(BF)
        return cc

    lax.fori_loop(0, 8, last, 0)
    for cp in (r0c, r1c, g0, g1, f0, f1):
        cp.wait_send()


def per_device(
    residual_input_stream, projected_queries, projected_keys, projected_values,
    emitted_switch_entries, retention_preactivations, additional_fading_amount, head_norm_gain,
    attention_output_weight, feedforward_norm_gain, gate_up_matrix, value_up_matrix,
    gate_filter_taps, value_filter_taps, down_projection_weight,
):
    lr = (
        jax.nn.log_sigmoid(retention_preactivations.astype(F32)) / 16.0
        + additional_fading_amount[:, None]
    )

    def woven(a, b):
        n = a.shape[0]
        both = jnp.stack([a.reshape(n, NT, 128), b.reshape(n, NT, 128)], axis=2)
        return both.reshape(n, 2 * HID)

    w = jnp.concatenate([woven(gate_up_matrix, value_up_matrix), down_projection_weight.T], axis=1)
    taps = woven(gate_filter_taps, value_filter_taps).astype(F32)
    anyspec = pl.BlockSpec(memory_space=pl.ANY)
    vspec = pl.BlockSpec(memory_space=pltpu.VMEM)
    dma = pltpu.SemaphoreType.DMA
    v = pltpu.VMEM
    return pl.pallas_call(
        body,
        out_shape=jax.ShapeDtypeStruct((CH, D), BF),
        in_specs=[anyspec] * 8 + [vspec] * 3,
        out_specs=vspec,
        scratch_shapes=[
            v((D, WCOLS), BF), v((1024, D), BF), v((ROWS, D), BF),
            v((ROWS, 128), BF), v((ROWS, 128), BF), v((ROWS, 256), BF), v((ROWS, 256), BF),
            v((ROWS, 128), F32), v((NB, 128, 128), F32), v((NB, 8, 128), F32),
            v((NB, 128, 128), BF), v((ROWS, 256), F32),
            v((2, 136, 128), F32), v((4, 136, 128), F32), v((4, 136, 128), F32),
            v((ROWS, 1024), BF), v((ROWS + HALO, D), BF), v((CH, D), F32), v((CH, D), F32),
            v((CH, HID), BF), v((4, CH, D), BF), v((2, CH, D // 2), BF), v((2, CH, D), BF),
            dma((8,)), dma((4, 15)), dma((4, 15)), dma((4, 15)), dma((4, 15)),
            dma((4,)), dma((4,)), dma((4,)), dma((4,)),
            dma((4,)), dma((3,)), dma((3,)), dma((3,)), dma((3,)),
            dma((4, 3)), dma((4, 3)), dma((2,)), dma((6,)), dma((6,)),
        ],
        compiler_params=pltpu.CompilerParams(
            collective_id=0, has_side_effects=True, vmem_limit_bytes=62 * 1024 * 1024
        ),
        name="layer",
    )(
        residual_input_stream, projected_queries, projected_keys, projected_values,
        emitted_switch_entries, lr, attention_output_weight, w,
        head_norm_gain[None], feedforward_norm_gain[None], taps,
    )


def solution(mesh):
    torus = Mesh(mesh.devices.reshape(4, 4, 2, mesh.shape["tp"]), (*SP, "tp"))
    return jax.shard_map(
        per_device,
        mesh=torus,
        in_specs=(
            P(SP, None), P(SP, "tp"), P(SP, "tp"), P(SP, "tp"), P(SP, "tp"), P(SP, "tp"),
            P(SP), P(), P("tp", None), P(), P(SP, "tp"), P(SP, "tp"), P(None, "tp"),
            P(None, "tp"), P("tp", SP),
        ),
        out_specs=P((*SP, "tp"), None),
        check_vma=False,
    )
```

time: 253 us -> 126 us (0.50); the launches traced: 250 us -> 125 us
  Pallas kernels: 0 us -> 116 us
  blocking collectives: 116 us -> 0 us
  waiting for transfers between devices: 40.1 us -> 0 us
  matrix products: 33.4 us -> 0 us
  other arithmetic: 19.1 us -> 1.95 us
  between operations: 13.7 us -> 0.08 us
  local copies, waits for them, and re-layouts: 18.1 us -> 7.09 us
  starting transfers between devices: 8.66 us -> 0 us
    pallas_call x0 -> x1, Pallas kernels: none -> 116 us  [per_device(): pl.pallas_call(body, out_shape=jax.ShapeDtypeStruct((CH, D), BF), in_spec...]
    all_to_all x3 -> x0, blocking collectives: 86.2 us -> none  [the longest x1 40.5 us: summed_on_arrival(): pieces = lax.all_to_all(split_up(array, dim, size), axis, 0, 0, tiled=True)]
    all_to_all x1 -> x0, waiting for transfers between devices: 39.3 us -> none  [copy_for_each(): lax.all_to_all(jnp.broadcast_to(array[None], (size, *array.shape)), axis,...]
    dot_general x9 -> x0, matrix products: 33.4 us -> none  [the longest x1 8.48 us: per_device(): gate_sum = jnp.dot(normed, pieces[0], preferred_element_type=jnp.float32)]
    all_gather x3 -> x0, blocking collectives: 30 us -> none  [all_in_one(): both, at, found = (lax.all_gather(jnp.concatenate(lines), axis), 0, {})]
    dynamic_update_slice x12 -> x0, other arithmetic: 7.69 us -> none  [per_device(): lax.scan(advance_recurrence, start_state, (jnp.exp(block_total), incremen...]
    all_to_all x1 -> x0, starting transfers between devices: 4.86 us -> none  [copy_for_each(): lax.all_to_all(jnp.broadcast_to(array[None], (size, *array.shape)), axis,...]
    transpose x1 -> x0, local copies, waits for them, and re-layouts: 4.68 us -> none  [all_blocks(): pieces.transpose(*turned, *range(len(order), pieces.ndim))]
  transfers between devices with their start and end apart: 6 -> 0, of which waited for: 1 -> 0; matrix products, arithmetic and copies ran while one was open for 24% -> 0% of each run, Pallas kernels for 0% -> 0%
where the time goes in v1:
time: 126 us; the launch traced here: 125 us
  Pallas kernels  116 us (92%)
  local copies, waits for them, and re-layouts  7.09 us (6%)
  other arithmetic  1.95 us (2%)
    pallas_call x1, Pallas kernels, per_device(): pl.pallas_call(body, out_shape=jax.ShapeDtypeStruct((CH, D), BF), in_spec...  116 us
    another operation x5, local copies, waits for them, and re-layouts, woven(): both = jnp.stack([a.reshape(n, NT, 128), b.reshape(n, NT, 128)], axis=2)  3.94 us

profile of v1, /device:TPU:0, one launch (start us, length us, event | category | flops | bytes accessed | tf_op | source)
XLA Modules:
  0.0 125.3 jit_solution(15772666932276450565)
XLA Ops:
  0.0 0.7 stack_reshape.14
  0.7 0.7 stack_reshape.15
  1.5 0.7 reshape.8.taps_ref
  2.2 1.0 stack_reshape.12
  3.2 1.1 stack_reshape.13
  4.3 0.0 copy-start.1
  4.3 0.1 pad_maximum_fusion.1
  4.4 0.4 copy.20
  4.8 0.0 copy-start
  4.8 0.0 copy-start.2
  4.8 0.1 reshape.7
  5.0 0.2 copy-done.1
  5.2 0.8 pad_maximum_fusion.w_hbm
  6.0 0.0 copy-done
  6.0 0.0 copy-done.2
  6.0 1.0 fusion.2.lr_hbm
  7.0 116.1 %layer.1 = bf16[192,2048]{1,0:T(8,128)(2,1)} custom-call(bf16[768,2048]{1,0:T(8,128)(2,1)} %x_hbm.1, bf16[768,128]{1,0:T(8,128)(2,1)} %q_hbm.1, bf16[768,128]{1,0:T(8,128)(2,1)} %k_hbm.1, bf16[768,256]{1,0:T(8,128)(2,1)} %v_hbm.1, bf16[768,256]{1,0:T(8,128)(2,1)} %g_hbm.1, f32[768,128]{1,0:T(8,128)} %fusion.2.lr_hbm, bf16[256,2048]{1,0:T(8,128)(2,1)} %wo_hbm.1, ...), custom_call_target="tpu_custom_call" | custom-call | tf_op jit(solution)/shard_map/layer/pallas_call | solution.py:510
  123.2 2.1 %copy.23 = bf16[192,2048]{1,0:T(8,128)(2,1)} copy(bf16[192,2048]{1,0:T(8,128)(2,1)} %layer.1) | data formatting | bytes 1572864
  (2 shorter events, 0.0 us)
Async XLA Ops:
  4.3 0.9 copy-start.1
  4.8 1.2 copy-start
  4.8 1.2 copy-start.2

commit v2 on v1

v2 whole, which is shorter than its diff:
```python
import jax
import jax.numpy as jnp
from jax import lax
from jax.experimental import pallas as pl
from jax.experimental.pallas import tpu as pltpu
from jax.sharding import Mesh
from jax.sharding import PartitionSpec as P

MESH = pl.DeviceIdType.MESH
BLOCK = 64
SP = ("sp_0", "sp_1", "sp_2")
EPS = 1e-06
BF = jnp.bfloat16
F32 = jnp.float32

ROWS = 768
D = 2048
HID = 1408
CH = 192
NCH = 4
NB = ROWS // BLOCK
GVW = 2 * HID
MAIN = 1280
HALFK = HID // 2
HALO = 16
OFF = (
    (0, 0), (-1, 0), (1, 0), (0, -1), (0, 1), (-1, -1), (1, 1), (1, -1), (-1, 1),
    (2, -1), (2, 1), (1, 2), (-1, 2), (2, 0), (0, 2), (2, 2),
)
VIA = (
    None, (-1, 0), (1, 0), (0, -1), (0, 1), (-1, 0), (1, 0), (0, -1), (0, 1),
    (-1, 0), (1, 0), (0, -1), (0, 1), (-1, 0), (0, -1), (0, 1),
)
SRC = (None, 0, 0, 0, 0, 3, 4, 2, 1, 5, 6, 7, 8, 1, 3, 10)
MIRROR = (0, 2, 1, 4, 3, 6, 5, 8, 7, 10, 9, 12, 11, 13, 14, 15)
QK = HALFK // 2
NT = HID // 128
STEPS = (
    ((), (1, 2, 3, 4)),
    ((1, 2, 3, 4), (5, 6, 7, 8)),
    ((5, 6, 7, 8), (9, 10, 11, 12, 13, 14)),
    ((9, 10, 11, 12), (15,)),
    ((13, 14, 15), ()),
)
CHUNKS = (3, 0, 1, 2)


def wrap(v):
    return lax.rem(v + 8, 4)


def rows_of(start, size):
    return pl.ds(pl.multiple_of(start, 16), size)


def nt_dot(a, b):
    return lax.dot_general(a, b, (((1,), (1,)), ((), ())), preferred_element_type=F32)


def tn_dot(a, b):
    return lax.dot_general(a, b, (((0,), (0,)), ((), ())), preferred_element_type=F32)


def body(
    x_hbm, q_hbm, k_hbm, v_hbm, g_hbm, r_hbm, wo_hbm, gw_hbm, vw_hbm, dw_hbm,
    fade_ref, hg_ref, fg_ref, gt_ref, vt_ref,
    out_ref,
    wgv, dbuf, dloc, dex, wobuf, xbuf, qbuf, kbuf, vbuf, gbuf, rbuf, rcb, tst, cbs, qst, outl,
    cbuf, ybuf, zbuf, mix, normed, resid, own, hid, parts, relay, fin,
    lsem, wsend, wrecv, dsend, drecv, osend, orecv, odsend, odrecv,
    csem, ysend, yrecv, zsend, zrecv, msend, mrecv, hsem, psend, precv,
):
    z, y, c, x = (lax.axis_index(n) for n in ("sp_0", "sp_1", "sp_2", "tp"))
    sp = z * 8 + y * 2 + c
    peer = 1 - c
    spn = lax.rem(sp + 1, 32)
    spp = lax.rem(sp + 31, 32)
    xr, xl, xo = wrap(x + 1), wrap(x - 1), wrap(x + 2)

    def at_sp(s):
        return {"sp_0": s // 8, "sp_1": lax.rem(s, 8) // 2, "sp_2": lax.rem(s, 2), "tp": x}

    def dev(dz=None, dy=None, dc=None, dx=None):
        return {
            "sp_0": z if dz is None else dz,
            "sp_1": y if dy is None else dy,
            "sp_2": c if dc is None else dc,
            "tp": x if dx is None else dx,
        }

    def remote(src, dst, ssem, rsem, to):
        return pltpu.make_async_remote_copy(
            src_ref=src, dst_ref=dst, send_sem=ssem, recv_sem=rsem, device_id=to,
            device_id_type=MESH,
        )

    barrier = pltpu.get_barrier_semaphore()
    partners = [dev(dc=peer), at_sp(spn), at_sp(spp), dev(dx=xr), dev(dx=xl)]
    for dlt in (1, 2, 3):
        partners += [dev(dy=wrap(y + dlt)), dev(dz=wrap(z + dlt))]
    for to in partners:
        pl.semaphore_signal(barrier, inc=1, device_id=to, device_id_type=MESH)

    mine = rows_of(sp * 64, 64)
    pairs = [
        (r_hbm, rbuf), (k_hbm, kbuf), (v_hbm, vbuf),
        (gw_hbm.at[:, 0:MAIN], wgv.at[mine, 0:MAIN]),
        (vw_hbm.at[:, 0:MAIN], wgv.at[mine, MAIN : 2 * MAIN]),
        (gw_hbm.at[:, MAIN:HID], wgv.at[mine, 2 * MAIN : 2 * MAIN + 128]),
        (vw_hbm.at[:, MAIN:HID], wgv.at[mine, 2 * MAIN + 128 : GVW]),
        (wo_hbm, wobuf.at[rows_of(x * 256, 256), :]),
        (dw_hbm, dloc), (q_hbm, qbuf), (g_hbm, gbuf), (x_hbm, xbuf),
    ]
    loads = [pltpu.make_async_copy(a, b, lsem.at[i]) for i, (a, b) in enumerate(pairs)]
    for cp in loads:
        cp.start()

    def shifted(off):
        dz, dy = off
        return wrap(z + dz), wrap(y + dy)

    def wref(pc, slot, cc):
        if pc >= 2:
            col = slot if pc == 2 else MIRROR[slot]
            return dbuf.at[rows_of(cc * HALFK + (pc - 2) * QK, QK), col * 128 : col * 128 + 128]
        dz, dy = OFF[slot]
        zz, yy = shifted((dz, dy) if pc == 0 else (-dz, -dy))
        return wgv.at[rows_of((zz * 8 + yy * 2 + cc) * 64 + pc * 32, 32), :]

    def wsendto(pc, r):
        vz, vy = VIA[r]
        src_slot = SRC[r]
        if pc >= 2 and r == 15:
            vz, vy = 1, 0
            src_slot = 11
        if pc % 2 == 1:
            vz, vy = -vz, -vy
        zz, yy = shifted((-vz, -vy))
        src = wref(pc, src_slot, c)
        dst = wref(pc, r, c) if pc >= 2 else src
        return remote(src, dst, wsend.at[pc, r], wrecv.at[pc, r], dev(dz=zz, dy=yy))

    def wpeer(pc, slot, cc):
        blk = wref(pc, slot, cc)
        return remote(blk, blk, dsend.at[pc, slot], drecv.at[pc, slot], dev(dc=peer))

    def wstep(pc, e):
        waits, sends = STEPS[e]
        for r in waits:
            blk = wref(pc, r, c)
            remote(blk, blk, wsend.at[pc, r], wrecv.at[pc, r], dev(dc=peer)).wait_recv()
        for r in sends:
            wsendto(pc, r).start()
        for r in waits or ((0,) if pc < 2 else ()):
            wpeer(pc, r, c).start()

    def ohalf(xx, cc):
        return wobuf.at[rows_of(xx * 256 + cc * 128, 128), :]

    def oquart(xx, cc, h):
        return wobuf.at[rows_of(xx * 256 + cc * 128 + h * 64, 64), :]

    lane = lax.broadcasted_iota(jnp.int32, (1, 128), 1)
    low = lane < 64
    ri = lax.broadcasted_iota(jnp.int32, (64, 64), 0)
    ci = lax.broadcasted_iota(jnp.int32, (64, 64), 1)
    li = lax.broadcasted_iota(jnp.int32, (64, 128), 1) - lax.broadcasted_iota(jnp.int32, (64, 128), 0)
    tri = (ri >= ci).astype(F32)
    for cp in loads[:3]:
        cp.wait()

    def state_step(n, carry):
        st, cb = carry
        rows = rows_of(n * 64, 64)
        fr = jnp.where(li == 64 * lax.rem(n, 2), fade_ref[pl.ds(n // 2, 1), :], 0.0)
        r = rbuf[rows, :].astype(F32)
        soft = jnp.maximum(-r, 0.0) + jnp.log1p(jnp.exp(-jnp.abs(r)))
        lr = jnp.sum(fr, axis=-1, keepdims=True) - soft * (1.0 / 16.0)
        rc = jnp.dot(tri, lr, precision=lax.Precision.HIGHEST, preferred_element_type=F32)
        rcb[rows, :] = rc
        bt = rc[63:64, :]
        kf = (kbuf[rows, :].astype(F32) * jnp.exp(bt - rc)).astype(BF)
        pr = tn_dot(vbuf[rows, :], kf)
        tst[n] = st
        cbs[n] = jnp.broadcast_to(cb, (8, 128))
        st = jnp.exp(bt) * st + jnp.where(low, pr[:128], pr[128:])
        return st, cb + bt

    def states(first, carry):
        for n in range(4):
            carry = state_step(first + n, carry)
        return carry

    carry = states(0, (jnp.zeros((128, 128), F32), jnp.zeros((1, 128), F32)))
    pl.semaphore_wait(barrier, len(partners))
    for cp in loads[3:7]:
        cp.wait()
    wstep(0, 0)
    loads[7].wait()
    o0 = remote(ohalf(x, c), ohalf(x, c), osend.at[0], orecv.at[0], dev(dx=xr))
    o1 = remote(ohalf(x, c), ohalf(x, c), osend.at[1], orecv.at[1], dev(dx=xl))
    o0.start()
    o1.start()
    st, la = lax.fori_loop(1, 3, lambda i, a: states(4 * i, a), carry)
    def put_state(ref, s_, l_):
        ref[0:128, :] = s_.astype(BF)
        hi = l_.astype(BF).astype(F32)
        mid = (l_ - hi).astype(BF).astype(F32)
        rr = lax.broadcasted_iota(jnp.int32, (16, 128), 0)
        ref[128:144, :] = jnp.where(
            rr == 0, hi, jnp.where(rr == 1, mid, jnp.where(rr == 2, l_ - hi - mid, 0.0))
        ).astype(BF)

    def get_state(ref):
        return ref[0:128, :].astype(F32), jnp.sum(ref[128:144, :].astype(F32), axis=0, keepdims=True)

    put_state(cbuf.at[0], st, la)
    cx = remote(cbuf.at[0], cbuf.at[1], csem.at[0], csem.at[1], dev(dc=peer))
    cx.start()
    loads[8].wait()
    dx = remote(dloc, dex, csem.at[2], csem.at[3], dev(dc=peer))
    dx.start()
    loads[9].wait()

    def within_step(n):
        rows = rows_of(n * 64, 64)
        rc = rcb[rows, :]
        qd = qbuf[rows, :].astype(F32) * 0.125 * jnp.exp(rc)
        kg = (kbuf[rows, :].astype(F32) * jnp.exp(-rc)).astype(BF)
        zero = jnp.zeros_like(qd)
        qq = jnp.concatenate([jnp.where(low, qd, zero), jnp.where(low, zero, qd)], axis=0).astype(BF)
        qst[n] = qq
        sc = nt_dot(qq, kg)
        s0 = jnp.where(ri >= ci, sc[:64], 0.0).astype(BF)
        s1 = jnp.where(ri >= ci, sc[64:], 0.0).astype(BF)
        vv = vbuf[rows, :]
        outl[rows, 0:128] = jnp.dot(s0, vv[:, :128], preferred_element_type=F32)
        outl[rows, 128:256] = jnp.dot(s1, vv[:, 128:], preferred_element_type=F32)

    def within(first):
        for n in range(4):
            within_step(first + n)

    within(0)
    cx.wait()
    other, ola = get_state(cbuf.at[1])
    second = c == 1
    s_first = jnp.where(second, other, st)
    s_second = jnp.where(second, st, other)
    la_second = jnp.where(second, la, ola)
    pc = jnp.where(second, other, jnp.zeros_like(other))
    pc_la = jnp.where(second, ola, jnp.zeros_like(ola))
    chip = jnp.exp(la_second) * s_first + s_second
    chip_la = la + ola

    def ring_scan(buf, ssem, rsem, me, value, value_la, to, cover):
        put_state(buf.at[me], value, value_la)
        sent = [
            remote(buf.at[me], buf.at[me], ssem.at[dlt - 1], rsem.at[dlt - 1], to(wrap(me + dlt)))
            for dlt in (1, 2, 3)
        ]
        for cp in sent:
            cp.start()
        cover()
        for dlt in (1, 2, 3):
            src = buf.at[wrap(me - dlt)]
            remote(src, src, ssem.at[dlt - 1], rsem.at[dlt - 1], to(wrap(me + dlt))).wait_recv()
        tot = jnp.zeros((128, 128), F32)
        tot_la = jnp.zeros((1, 128), F32)
        pre, pre_la = tot, tot_la
        for k in range(4):
            tk, lk = get_state(buf.at[k])
            tot = jnp.exp(lk) * tot + tk
            tot_la = tot_la + lk
            passed = k < me
            pre = jnp.where(passed, tot, pre)
            pre_la = jnp.where(passed, tot_la, pre_la)
        return pre, pre_la, tot, tot_la, sent

    def cover_y():
        wstep(1, 0)
        within(4)

    def join_down():
        dx.wait_recv()

        def one(j, cc):
            cs = pl.ds(pl.multiple_of(j * 128, 128), 128)
            a = dloc[:, cs].astype(F32)
            b = dex[:, cs].astype(F32)
            both = jnp.concatenate([jnp.where(c == 1, b, a), jnp.where(c == 1, a, b)], axis=0)
            dbuf[rows_of(j * 128, 128), 0:128] = both.T.astype(BF)
            return cc

        lax.fori_loop(0, NT, one, 0)

    def cover_z():
        wstep(0, 1)
        within(8)
        join_down()

    py, py_la, tot, tot_la, ysent = ring_scan(
        ybuf, ysend, yrecv, y, chip, chip_la, lambda k: dev(dy=k), cover_y
    )
    pz, pz_la, tot, tot_la, zsent = ring_scan(
        zbuf, zsend, zrecv, z, tot, tot_la, lambda k: dev(dz=k), cover_z
    )
    tin = jnp.exp(pc_la) * (jnp.exp(py_la) * pz + py) + pc
    loads[10].wait()

    mlane = pl.multiple_of(x * 256, 256)

    def mix_step(n):
        rows = rows_of(n * 64, 64)
        full = (tst[n] + jnp.exp(cbs[n][0:1, :]) * tin).astype(BF)
        e = nt_dot(qst[n], full)
        got = []
        for h in range(2):
            o = outl[rows, h * 128 : h * 128 + 128] + e[h * 64 : h * 64 + 64]
            o = o * lax.rsqrt(jnp.mean(o * o, axis=-1, keepdims=True) + EPS) * hg_ref[...]
            gt = gbuf[rows, h * 128 : h * 128 + 128].astype(F32)
            got.append(o * (gt / (1.0 + jnp.exp(-gt))))
        mix[rows, pl.ds(mlane, 256)] = jnp.concatenate(got, axis=1).astype(BF)

    def mblock(h, xx):
        return mix.at[h * CH : h * CH + CH, pl.ds(pl.multiple_of(xx * 256, 256), 256)]

    msent = []

    def mix_chunk(h):
        for n in range(3):
            mix_step(h * 3 + n)
        for j, to in ((0, xr), (1, xl)):
            cp = remote(mblock(h, x), mblock(h, x), msend.at[h, j], mrecv.at[h, j], dev(dx=to))
            cp.start()
            msent.append(cp)

    def mwait(h, j, xx):
        remote(mblock(h, xx), mblock(h, xx), msend.at[h, j], mrecv.at[h, j], dev(dx=xr)).wait_recv()

    def mrelay(h):
        mwait(h, 0, xl)
        mwait(h, 1, xr)
        src, to = (xl, xr) if h % 2 == 0 else (xr, xl)
        cp = remote(mblock(h, src), mblock(h, src), msend.at[h, 2], mrecv.at[h, 2], dev(dx=to))
        cp.start()
        msent.append(cp)

    mix_chunk(3)
    mix_chunk(0)
    wstep(1, 1)
    remote(ohalf(xl, c), ohalf(xl, c), osend.at[0], orecv.at[0], dev(dx=xr)).wait_recv()
    o2 = remote(oquart(xl, c, 0), oquart(xl, c, 0), osend.at[2], orecv.at[2], dev(dx=xr))
    o2.start()
    remote(ohalf(xr, c), ohalf(xr, c), osend.at[1], orecv.at[1], dev(dx=xl)).wait_recv()
    o3 = remote(oquart(xr, c, 1), oquart(xr, c, 1), osend.at[3], orecv.at[3], dev(dx=xl))
    o3.start()
    od = [
        remote(r, r, odsend.at[i], odrecv.at[i], dev(dc=peer))
        for i, r in enumerate((ohalf(xl, c), ohalf(xr, c), oquart(xo, c, 0), oquart(xo, c, 1)))
    ]
    od[0].start()
    od[1].start()
    wstep(0, 2)
    mrelay(3)
    mrelay(0)
    mix_chunk(1)
    mix_chunk(2)
    wstep(1, 2)
    remote(oquart(xo, c, 0), oquart(xo, c, 0), osend.at[2], orecv.at[2], dev(dx=xr)).wait_recv()
    od[2].start()
    remote(oquart(xo, c, 1), oquart(xo, c, 1), osend.at[3], orecv.at[3], dev(dx=xl)).wait_recv()
    od[3].start()
    wstep(0, 3)
    wstep(2, 0)
    for i, r in enumerate((ohalf(xl, peer), ohalf(xr, peer), oquart(xo, peer, 0), oquart(xo, peer, 1))):
        remote(r, r, odsend.at[i], odrecv.at[i], dev(dc=peer)).wait_recv()
    loads[11].wait()

    def chunk_norm(h):
        r0 = h * CH
        ss = jnp.zeros((CH, 128), F32)
        for i in range(2):
            cs = slice(i * 1024, i * 1024 + 1024)
            a = jnp.dot(mix[r0 : r0 + CH, :], wobuf[:, cs], preferred_element_type=F32)
            a = a + xbuf[r0 : r0 + CH, cs].astype(F32)
            resid[:, cs] = a
            sq = a * a
            for b in range(8):
                ss = ss + sq[:, b * 128 : b * 128 + 128]
        rs = lax.rsqrt(jnp.sum(ss, axis=-1, keepdims=True) * (1.0 / D) + EPS)

        def norm(i, carry):
            cs = pl.ds(pl.multiple_of(i * 256, 256), 256)
            normed[HALO + r0 : HALO + r0 + CH, cs] = (resid[:, cs] * rs * fg_ref[:, cs]).astype(BF)
            return carry

        lax.fori_loop(0, 8, norm, 0)

        @pl.when(x == h)
        def _():
            def keep(i, carry):
                cs = pl.ds(pl.multiple_of(i * 256, 256), 256)
                own[:, cs] = resid[:, cs]
                return carry

            lax.fori_loop(0, 8, keep, 0)

    tail = normed.at[ROWS : ROWS + HALO, :]
    halo = normed.at[0:HALO, :]
    hcopy = remote(tail, halo, hsem.at[0], hsem.at[1], at_sp(spn))

    def norm_of(h):
        mwait(h, 2, xo)
        chunk_norm(h)

    norm_of(3)
    hcopy.start()
    norm_of(0)
    mrelay(1)
    wstep(1, 3)
    wstep(3, 0)
    mrelay(2)
    wstep(0, 4)
    norm_of(1)
    norm_of(2)
    wstep(2, 1)
    wstep(1, 4)
    hcopy.wait()

    @pl.when(sp == 0)
    def _():
        normed[0:HALO, :] = jnp.zeros((HALO, D), BF)

    for pc_ in range(2):
        for r in range(16):
            wpeer(pc_, r, peer).wait_recv()

    def up(i, h, mid=lambda: None):
        win = rows_of(h * CH, CH + HALO)

        def mixed_taps(u, taps):
            u = u.astype(BF).astype(F32)
            m = taps[0:1] * pltpu.roll(u, 2, 0) + taps[1:2] * pltpu.roll(u, 1, 0) + taps[2:3] * u
            return m[HALO:]

        def act(gm, vm):
            return (gm / (1.0 + jnp.exp(-gm)) * vm).astype(BF)

        for j in range(5):
            cs = slice(j * 256, j * 256 + 256)
            vs = slice(MAIN + j * 256, MAIN + j * 256 + 256)
            a = jnp.dot(normed[win, :], wgv[:, cs], preferred_element_type=F32)
            b = jnp.dot(normed[win, :], wgv[:, vs], preferred_element_type=F32)
            gm = mixed_taps(a, gt_ref[:, cs].astype(F32))
            vm = mixed_taps(b, vt_ref[:, cs].astype(F32))
            hid[i, :, cs] = act(gm, vm)
            if j == 2:
                mid()
        a = jnp.dot(normed[win, :], wgv[:, 2 * MAIN : GVW], preferred_element_type=F32)
        gm = mixed_taps(a[:, :128], gt_ref[:, MAIN:HID].astype(F32))
        vm = mixed_taps(a[:, 128:], vt_ref[:, MAIN:HID].astype(F32))
        hid[i, :, MAIN:HID] = act(gm, vm)

    def quarter(g):
        return slice(g * 512, g * 512 + 512)

    def down(i, g, add=False):
        a = jnp.dot(hid[i], dbuf[:, quarter(g)], preferred_element_type=F32)
        if add:
            a = a + relay[g].astype(F32)
        parts[i, :, quarter(g)] = a.astype(BF)

    def rs_copy(kind, g):
        if kind == 0:
            return remote(
                parts.at[0, :, quarter(g)], relay.at[g], psend.at[0, g], precv.at[0, g],
                dev(dx=xr if g in (0, 3) else xl),
            )
        return remote(
            parts.at[kind, :, quarter(g)], fin.at[kind - 1, :, quarter(g)], psend.at[kind, g],
            precv.at[kind, g], dev(dx=xr if kind == 1 else xl),
        )

    def dpeer(slots):
        for pc_ in (2, 3):
            for r in slots:
                wpeer(pc_, r, peer).wait_recv()

    def send_down(kind, g, relayed=False):
        if relayed:
            rs_copy(0, g).wait_recv()
        down(kind, g, relayed)
        rs_copy(kind, g).start()

    def first_sends():
        wstep(2, 2)
        wstep(3, 2)
        dpeer(range(1, 9))
        send_down(0, 0)
        send_down(0, 1)

    def third_quarter():
        wstep(3, 3)
        dpeer(range(9, 13))
        send_down(0, 2)

    up(0, xo, lambda: wstep(3, 1))
    up(1, xr, first_sends)
    send_down(1, 1)
    wstep(2, 3)
    up(2, xl, third_quarter)
    send_down(2, 0)
    send_down(1, 0, True)
    send_down(2, 1, True)
    wstep(2, 4)
    wstep(3, 4)
    dpeer(range(13, 16))
    send_down(0, 3)
    send_down(1, 2)
    send_down(2, 3)
    up(3, x)
    send_down(2, 2, True)
    for g in range(4):
        down(3, g)
    send_down(1, 3, True)

    for pc_ in range(4):
        for r in range(1, 16):
            wsendto(pc_, r).wait_send()
        for r in range(0 if pc_ < 2 else 1, 16):
            wpeer(pc_, r, c).wait_send()
    dx.wait_send()
    for cp in (o0, o1, o2, o3, *od, *ysent, *zsent, *msent):
        cp.wait_send()
    for g in (1, 0, 2, 3):
        rs_copy(1, g).wait_recv()
    for g in (0, 1, 3, 2):
        rs_copy(2, g).wait_recv()
    for s in range(16):
        zz, yy = shifted(OFF[s])
        cs = pl.ds(pl.multiple_of((zz * 4 + yy) * 128, 128), 128)
        ls = slice(s * 128, s * 128 + 128)
        a = own[:, cs] + parts[3, :, ls].astype(F32)
        a = a + (fin[0, :, ls].astype(F32) + fin[1, :, ls].astype(F32))
        out_ref[:, cs] = a.astype(BF)
    for kind in range(3):
        for g in range(4):
            rs_copy(kind, g).wait_send()


def per_device(
    residual_input_stream, projected_queries, projected_keys, projected_values,
    emitted_switch_entries, retention_preactivations, additional_fading_amount, head_norm_gain,
    attention_output_weight, feedforward_norm_gain, gate_up_matrix, value_up_matrix,
    gate_filter_taps, value_filter_taps, down_projection_weight,
):
    anyspec = pl.BlockSpec(memory_space=pl.ANY)
    vspec = pl.BlockSpec(memory_space=pltpu.VMEM)
    dma = pltpu.SemaphoreType.DMA
    v = pltpu.VMEM
    return pl.pallas_call(
        body,
        out_shape=jax.ShapeDtypeStruct((CH, D), BF),
        in_specs=[anyspec] * 10 + [vspec] * 5,
        out_specs=vspec,
        scratch_shapes=[
            v((D, GVW), BF), v((HID, D), BF), v((64, HID), BF), v((64, HID), BF),
            v((1024, D), BF), v((ROWS, D), BF),
            v((ROWS, 128), BF), v((ROWS, 128), BF), v((ROWS, 256), BF), v((ROWS, 256), BF),
            v((ROWS, 128), BF), v((ROWS, 128), F32), v((NB, 128, 128), F32), v((NB, 8, 128), F32),
            v((NB, 128, 128), BF), v((ROWS, 256), F32),
            v((2, 144, 128), BF), v((4, 144, 128), BF), v((4, 144, 128), BF),
            v((ROWS, 1024), BF), v((ROWS + HALO, D), BF), v((CH, D), F32), v((CH, D), F32),
            v((4, CH, HID), BF), v((4, CH, D), BF), v((4, CH, 512), BF), v((2, CH, D), BF),
            dma((12,)), dma((4, 16)), dma((4, 16)), dma((4, 16)), dma((4, 16)),
            dma((4,)), dma((4,)), dma((4,)), dma((4,)),
            dma((4,)), dma((3,)), dma((3,)), dma((3,)), dma((3,)),
            dma((4, 3)), dma((4, 3)), dma((2,)), dma((3, 4)), dma((3, 4)),
        ],
        compiler_params=pltpu.CompilerParams(
            collective_id=0, has_side_effects=True, vmem_limit_bytes=62 * 1024 * 1024
        ),
        name="layer",
    )(
        residual_input_stream, projected_queries, projected_keys, projected_values,
        emitted_switch_entries, retention_preactivations, attention_output_weight,
        gate_up_matrix, value_up_matrix, down_projection_weight.T,
        additional_fading_amount.reshape(ROWS // 128, 128), head_norm_gain[None],
        feedforward_norm_gain[None], gate_filter_taps, value_filter_taps,
    )


def solution(mesh):
    torus = Mesh(mesh.devices.reshape(4, 4, 2, mesh.shape["tp"]), (*SP, "tp"))
    return jax.shard_map(
        per_device,
        mesh=torus,
        in_specs=(
            P(SP, None), P(SP, "tp"), P(SP, "tp"), P(SP, "tp"), P(SP, "tp"), P(SP, "tp"),
            P(SP), P(), P("tp", None), P(), P(SP, "tp"), P(SP, "tp"), P(None, "tp"),
            P(None, "tp"), P("tp", SP),
        ),
        out_specs=P((*SP, "tp"), None),
        check_vma=False,
    )
```

time: 126 us -> 93.5 us (0.74)
  Pallas kernels: 116 us -> 90.6 us
  local copies, waits for them, and re-layouts: 7.09 us -> 2.09 us
  other arithmetic: 1.95 us -> 0 us
    pallas_call x1, Pallas kernels: 116 us -> 90.6 us  [per_device(): pl.pallas_call(body, out_shape=jax.ShapeDtypeStruct((CH, D), BF), in_spec...]
    another operation x5 -> x0, local copies, waits for them, and re-layouts: 3.94 us -> none  [woven(): both = jnp.stack([a.reshape(n, NT, 128), b.reshape(n, NT, 128)], axis=2)]
where the time goes in v2:
time: 93.5 us; the launch traced here: 92.6 us
  Pallas kernels  90.6 us (97%)
  local copies, waits for them, and re-layouts  2.09 us (2%)
    pallas_call x1, Pallas kernels, per_device(): pl.pallas_call(body, out_shape=jax.ShapeDtypeStruct((CH, D), BF), in_spec...  90.6 us
    unnamed x1, local copies, waits for them, and re-layouts  2.09 us

profile of v2, /device:TPU:0, one launch (start us, length us, event | category | flops | bytes accessed | tf_op | source)
XLA Modules:
  0.0 92.6 jit_solution(9492235203890449330)
XLA Ops:
  0.0 90.6 %layer.1 = bf16[192,2048]{1,0:T(8,128)(2,1)} custom-call(bf16[768,2048]{1,0:T(8,128)(2,1)} %x_hbm.1, bf16[768,128]{1,0:T(8,128)(2,1)} %q_hbm.1, bf16[768,128]{1,0:T(8,128)(2,1)} %k_hbm.1, bf16[768,256]{1,0:T(8,128)(2,1)} %v_hbm.1, bf16[768,256]{1,0:T(8,128)(2,1)} %g_hbm.1, bf16[768,128]{1,0:T(8,128)(2,1)} %r_hbm.1, bf16[256,2048]{1,0:T(8,128)(2,1)} %wo_hbm.1, ...), custom_call_target="tpu_custom_call" | custom-call | tf_op jit(solution)/shard_map/layer/pallas_call | solution.py:562
  90.6 2.1 %copy.17 = bf16[192,2048]{1,0:T(8,128)(2,1)} copy(bf16[192,2048]{1,0:T(8,128)(2,1)} %layer.1) | data formatting | bytes 1572864
